TPU v7x, 32 devices: a whole 2x2x4 slice. The times are simulated.
32 devices in a mesh: grp: 2 (over y), fs: 4 (over z), tp: 4 (over x, core).
Axes of the slice: x: 2, y: 2, z: 4, core: 2. Of those that a mesh axis runs over, the one named last changes fastest.
Arguments:
- tokens: bfloat16 [2048, 2048], P(('grp', 'fs'), 'tp'), parts along dimension 0, may hold values from -6 to 6
- recurrent_norm_gain: float32 [2048], replicated, may hold values from 0.1 to 1.9
- feedforward_norm_gain: float32 [2048], replicated, may hold values from 0.1 to 1.9
- gate_projection_weight: bfloat16 [2048, 2048], P('fs', 'tp'), may hold values from -0.125 to 0.125
- recurrent_projection_weight: bfloat16 [2048, 2048], P('fs', 'tp'), may hold values from -0.125 to 0.125
- convolution_kernel: bfloat16 [4, 2048], P(None, 'tp'), may hold values from -3 to 3
- decay_gate_matrix: bfloat16 [16, 128, 128], P('tp'), may hold values from -0.5 to 0.5
- input_gate_matrix: bfloat16 [16, 128, 128], P('tp'), may hold values from -0.5 to 0.5
- base_decay_logit: float32 [2048], P('tp'), may hold values from 3 to 9
- extra_log_decay: float32 [2048], P(('grp', 'fs')), parts along dimension 0, may hold values from -0.7 to 0
- output_projection_weight: bfloat16 [2048, 2048], P('tp', 'fs'), may hold values from -0.125 to 0.125
- up_projection_weight: bfloat16 [2048, 8192], P('fs', 'tp'), may hold values from -0.125 to 0.125
- down_projection_weight: bfloat16 [8192, 2048], P('tp', 'fs'), may hold values from -0.0625 to 0.0625
Outputs:
- layer_out: bfloat16 [2048, 2048], P(('grp', 'fs'), 'tp'), parts along dimension 0
There are 2 independent parts, one for each index of `grp`. A program takes and returns all parts, laid end to end along the dimension named above; an argument that names none is the same for every part. Nothing has to cross between parts.
All inputs are finite; a program needn't handle non-finite values.
Results may differ from a plain program's by a relative error of at most 0.018.
Values may be sent and summed in bfloat16 or wider, within the bound.
A program may use at most 64 MiB of HBM per device.

v0:
```python
import jax
import jax.numpy as jnp
from jax import lax
from jax.sharding import PartitionSpec as P


def rms_rows(values_in, norm_gain):
    values = values_in.astype(jnp.float32)
    inverse = lax.rsqrt(jnp.mean(values * values, axis=-1, keepdims=True) + 1e-06)
    return (values * inverse * norm_gain).astype(jnp.bfloat16)


def combine(earlier, later):
    return (earlier[0] * later[0], later[0] * earlier[1] + later[1])


def recurrent_state(
    recurrent_branch_rows,
    gate_branch_rows,
    convolution_kernel,
    decay_gate_matrix,
    input_gate_matrix,
    base_decay_logit,
    extra_log_decay,
):
    length = recurrent_branch_rows.shape[0]
    taps = convolution_kernel.shape[0]
    padded = jnp.pad(recurrent_branch_rows.astype(jnp.float32), ((taps - 1, 0), (0, 0)))
    conv_sum = jnp.zeros((length, recurrent_branch_rows.shape[1]), jnp.float32)
    for tap_index in range(taps):
        conv_sum = conv_sum + padded[tap_index : tap_index + length] * convolution_kernel[
            tap_index
        ].astype(jnp.float32)
    conv_rows = conv_sum.astype(jnp.bfloat16)
    blocks = decay_gate_matrix.shape[0]
    blocked = conv_rows.reshape(length, blocks, -1)
    recurrence_gate = jax.nn.sigmoid(
        jnp.einsum(
            "tni,nij->tnj", blocked, decay_gate_matrix, preferred_element_type=jnp.float32
        ).reshape(length, -1)
    )
    input_rate = jax.nn.sigmoid(
        jnp.einsum(
            "tni,nij->tnj", blocked, input_gate_matrix, preferred_element_type=jnp.float32
        ).reshape(length, -1)
    )
    decay_log_values = (
        -8.0 * jax.nn.softplus(-base_decay_logit) * recurrence_gate + extra_log_decay[:, None]
    )
    decay = jnp.exp(decay_log_values)
    drive = (
        jnp.sqrt(-jnp.expm1(2.0 * decay_log_values)) * input_rate * conv_rows.astype(jnp.float32)
    )
    _, hidden = lax.associative_scan(combine, (decay, drive), axis=0)
    return (hidden * gate_branch_rows.astype(jnp.float32)).astype(jnp.bfloat16)


def per_device(
    tokens,
    recurrent_norm_gain,
    feedforward_norm_gain,
    gate_projection_weight,
    recurrent_projection_weight,
    convolution_kernel,
    decay_gate_matrix,
    input_gate_matrix,
    base_decay_logit,
    extra_log_decay,
    output_projection_weight,
    up_projection_weight,
    down_projection_weight,
):
    whole_rows = lax.all_gather(tokens, "tp", axis=1, tiled=True)
    normed = rms_rows(whole_rows, recurrent_norm_gain)
    columns = normed
    gate_pre = jnp.dot(
        columns,
        lax.all_gather(gate_projection_weight, "fs", axis=0, tiled=True),
        preferred_element_type=jnp.float32,
    )
    recur_pre = jnp.dot(
        columns,
        lax.all_gather(recurrent_projection_weight, "fs", axis=0, tiled=True),
        preferred_element_type=jnp.float32,
    )
    gate_branch_rows = jax.nn.gelu(gate_pre).astype(jnp.bfloat16)
    recurrent_branch_rows = recur_pre.astype(jnp.bfloat16)
    mixed_output = recurrent_state(
        recurrent_branch_rows,
        gate_branch_rows,
        convolution_kernel,
        decay_gate_matrix,
        input_gate_matrix,
        base_decay_logit,
        extra_log_decay,
    )
    partials = jnp.dot(
        mixed_output,
        lax.all_gather(output_projection_weight, "fs", axis=1, tiled=True),
        preferred_element_type=jnp.float32,
    )
    residual = (
        tokens.astype(jnp.float32)
        + lax.psum_scatter(
            partials.astype(jnp.bfloat16), "tp", scatter_dimension=1, tiled=True
        ).astype(jnp.float32)
    ).astype(jnp.bfloat16)
    middle = lax.all_gather(residual, "tp", axis=1, tiled=True)
    channel_in = rms_rows(middle, feedforward_norm_gain)
    columns = channel_in
    upward = jnp.dot(
        columns,
        lax.all_gather(up_projection_weight, "fs", axis=0, tiled=True),
        preferred_element_type=jnp.float32,
    )
    positive = jnp.maximum(upward, 0.0)
    squared = (positive * positive).astype(jnp.bfloat16)
    down_terms = jnp.dot(
        squared,
        lax.all_gather(down_projection_weight, "fs", axis=1, tiled=True),
        preferred_element_type=jnp.float32,
    )
    summed_down = lax.psum_scatter(
        down_terms.astype(jnp.bfloat16), "tp", scatter_dimension=1, tiled=True
    ).astype(jnp.float32)
    return (residual.astype(jnp.float32) + summed_down).astype(jnp.bfloat16)


def solution(mesh):
    placed = (
        P(("grp", "fs"), "tp"),
        P(),
        P(),
        P("fs", "tp"),
        P("fs", "tp"),
        P(None, "tp"),
        P("tp", None, None),
        P("tp", None, None),
        P("tp"),
        P(("grp", "fs")),
        P("tp", "fs"),
        P("fs", "tp"),
        P("tp", "fs"),
    )
    return jax.shard_map(
        per_device, mesh=mesh, in_specs=placed, out_specs=P(("grp", "fs"), "tp"), check_vma=False
    )
```

profile of v0, /device:TPU:0, one launch (start us, length us, event | category | flops | bytes accessed | tf_op | source)
XLA Modules:
  0.0 558.3 jit_solution(17213416898491841167)
XLA Ops:
  6.5 0.7 all-gather.8.cloned.1.call-update
  7.3 0.0 all-gather.10.cloned.1.call-start
  7.3 0.7 all-gather.10.cloned.1.call-update
  8.0 0.0 all-gather.12.cloned.1.call-start
  8.1 0.7 all-gather.12.cloned.1.call-update
  8.7 0.0 all-gather.14.cloned.1.call-start
  8.8 0.5 all-gather.14.cloned.1.call-update
  9.3 0.0 reduce-scatter.3.cloned.1.call-start
  9.4 0.8 slice_convert_fusion.3
  10.2 0.7 fusion.55
  10.9 17.4 %all-gather.8.cloned.1.call-done = bf16[256,2048]{1,0:T(8,128)(2,1)} async-done(((bf16[256,512]{1,0:T(8,128)(2,1)}), bf16[256,2048]{1,0:T(8,128)(2,1)}) %all-gather.8.cloned.1.call-update) | async-done | bytes 1048592 | tf_op jit(solution)/shard_map/all_gather | solution.py:73
  28.4 1.5 fusion.2
  29.9 45.7 %all-gather.10.cloned.1.call-done = bf16[2048,512]{1,0:T(8,128)(2,1)} async-done(((bf16[512,512]{1,0:T(8,128)(2,1)}), bf16[2048,512]{1,0:T(8,128)(2,1)}) %all-gather.10.cloned.1.call-update) | async-done | bytes 2097168 | tf_op jit(solution)/shard_map/all_gather | solution.py:83
  75.6 2.7 fusion.14
  78.3 0.0 copy-start.5
  78.3 0.2 fusion.77
  78.6 0.0 copy-done
  78.6 0.3 fusion.11
  78.9 0.0 copy-start.4
  78.9 0.2 copy.22
  79.1 0.1 copy-done.5
  79.2 0.3 fusion.13
  79.5 0.2 copy.23
  79.8 0.7 fusion.29
  80.4 0.3 slice.215
  80.8 0.3 slice.216
  81.1 0.3 slice.214
  81.4 0.3 slice.218
  81.7 0.1 fusion.62
  81.8 0.1 slice.221
  82.0 0.1 slice.222
  82.1 0.1 slice.220
  82.2 0.1 slice.224
  83.1 0.2 slice.219
  83.3 0.2 slice.268
  83.5 0.3 slice.270
  83.9 0.3 slice.213
  84.9 0.1 pad.69
  85.0 0.1 fusion.41
  85.1 0.1 pad.68
  85.2 0.0 copy-start.2
  85.2 36.4 %all-gather.12.cloned.1.call-done = bf16[2048,512]{1,0:T(8,128)(2,1)} async-done(((bf16[512,512]{1,0:T(8,128)(2,1)}), bf16[2048,512]{1,0:T(8,128)(2,1)}) %all-gather.12.cloned.1.call-update) | async-done | bytes 2097168 | tf_op jit(solution)/shard_map/all_gather | solution.py:78
  121.7 45.9 %all-gather.14.cloned.1.call-done = bf16[512,2048]{1,0:T(8,128)(2,1)} async-done(((bf16[512,512]{1,0:T(8,128)(2,1)}), bf16[512,2048]{1,0:T(8,128)(2,1)}) %all-gather.14.cloned.1.call-update) | async-done | bytes 2097168 | tf_op jit(solution)/shard_map/all_gather | solution.py:99
  167.6 4.8 convolution_convert_fusion
  172.4 0.0 reduce-scatter.3.cloned.1.call-update
  172.4 0.0 all-gather.16.cloned.1.call-start
  172.5 23.7 %reduce-scatter.3.cloned.1.call-done = bf16[256,512]{1,0:T(8,128)(2,1)} async-done(((bf16[256,2048]{1,0:T(8,128)(2,1)}), bf16[256,512]{1,0:T(8,128)(2,1)}) %reduce-scatter.3.cloned.1.call-update) | async-done | bytes 262160 | tf_op jit(solution)/shard_map/reduce_scatter | solution.py:104
  196.1 1.7 add_convert_fusion.1
  197.9 0.0 all-gather.16.cloned.1.call-update
  197.9 0.0 all-gather.18.cloned.1.call-start
  197.9 0.7 all-gather.18.cloned.1.call-update
  198.6 0.0 copy-start.7
  198.6 0.0 all-gather.20.cloned.1.call-start
  198.7 0.7 all-gather.20.cloned.1.call-update
  199.4 0.0 reduce-scatter.5.cloned.1.call-start
  199.4 15.3 %all-gather.16.cloned.1.call-done = bf16[256,2048]{1,0:T(8,128)(2,1)} async-done(((bf16[256,512]{1,0:T(8,128)(2,1)}), bf16[256,2048]{1,0:T(8,128)(2,1)}) %all-gather.16.cloned.1.call-update) | async-done | bytes 1048592 | tf_op jit(solution)/shard_map/all_gather | solution.py:108
  214.7 1.5 fusion.5
  216.3 0.0 copy-start.1
  216.3 149.7 %all-gather.18.cloned.1.call-done = bf16[2048,2048]{1,0:T(8,128)(2,1)} async-done(((bf16[512,2048]{1,0:T(8,128)(2,1)}), bf16[2048,2048]{1,0:T(8,128)(2,1)}) %all-gather.18.cloned.1.call-update) | async-done | bytes 8388624 | tf_op jit(solution)/shard_map/all_gather | solution.py:113
  366.0 149.4 %all-gather.20.cloned.1.call-done = bf16[2048,2048]{1,0:T(8,128)(2,1)} async-done(((bf16[2048,512]{1,0:T(8,128)(2,1)}), bf16[2048,2048]{1,0:T(8,128)(2,1)}) %all-gather.20.cloned.1.call-update) | async-done | bytes 8388624 | tf_op jit(solution)/shard_map/all_gather | solution.py:120
  515.4 11.6 %convolution_convert_fusion.1 = bf16[256,2048]{1,0:T(8,128)(2,1)} fusion(bf16[2048,2048]{1,0:T(8,128)(2,1)} %all-gather.20.cloned.1.call-done, bf16[2048,2048]{1,0:T(8,128)(2,1)} %all-gather.18.cloned.1.call-done, bf16[256,2048]{1,0:T(8,128)(2,1)} %all-gather.16.cloned.1.call-done, f32[2048]{0:T(1024)S(1)} %copy-done.7, f32[256]{0:T(256)S(1)} %add_rsqrt_fusion), kind=kOutput, calls=%fused_computation.8 | convolution fusion | flops 4299161600 | bytes 18883584 | tf_op jit(solution)/shard_map/dot_general | solution.py:118
  527.0 0.0 reduce-scatter.5.cloned.1.call-update
  527.0 23.1 %reduce-scatter.5.cloned.1.call-done = bf16[256,512]{1,0:T(8,128)(2,1)} async-done(((bf16[256,2048]{1,0:T(8,128)(2,1)}), bf16[256,512]{1,0:T(8,128)(2,1)}) %reduce-scatter.5.cloned.1.call-update) | async-done | bytes 262160 | tf_op jit(solution)/shard_map/reduce_scatter | solution.py:123
  550.1 1.7 add_convert_fusion
  (85 shorter events, 1.3 us)
Async XLA Ops:
  6.5 72.0 %copy-start = (bf16[4,128,128]{2,1,0:T(8,128)(2,1)S(1)}, bf16[4,128,128]{2,1,0:T(8,128)(2,1)}, u32[]{:S(2)}) copy-start(bf16[4,128,128]{2,1,0:T(8,128)(2,1)} %param.19) | copy-start | bytes 393220
  6.5 69.1 %copy-start.6 = (f32[2048]{0:T(1024)S(1)}, f32[2048]{0:T(1024)}, u32[]{:S(2)}) copy-start(f32[2048]{0:T(1024)} %param.14) | copy-start | bytes 24580
  6.5 21.8 %all-gather.8.cloned.1.call-start = ((), (), s32[]{:S(2)}) async-start(), calls=%async_computation.2 | async-start | bytes 1310720 | tf_op jit(solution)/shard_map/all_gather | solution.py:73
  7.3 68.3 %all-gather.10.cloned.1.call-start = ((), (), s32[]{:S(2)}) async-start(), calls=%async_computation.3 | async-start | bytes 2621440 | tf_op jit(solution)/shard_map/all_gather | solution.py:83
  8.0 113.7 %all-gather.12.cloned.1.call-start = ((), (), s32[]{:S(2)}) async-start(), calls=%async_computation.4 | async-start | bytes 2621440 | tf_op jit(solution)/shard_map/all_gather | solution.py:78
  8.7 158.9 %all-gather.14.cloned.1.call-start = ((), (), s32[]{:S(2)}) async-start(), calls=%async_computation.5 | async-start | bytes 2621440 | tf_op jit(solution)/shard_map/all_gather | solution.py:99
  9.3 186.8 %reduce-scatter.3.cloned.1.call-start = ((), (), s32[]{:S(2)}) async-start(), calls=%async_computation.6 | async-start | bytes 1310720 | tf_op jit(solution)/shard_map/reduce_scatter | solution.py:104
  78.3 0.9 copy-start.5
  78.9 0.8 copy-start.4
  84.9 82.7 %copy-start.3 = (bf16[256,2048]{1,0:T(8,128)(2,1)S(1)}, bf16[256,2048]{1,0:T(8,128)(2,1)}, u32[]{:S(2)}) copy-start(bf16[256,2048]{1,0:T(8,128)(2,1)} %all-gather.8.cloned.1.call-done) | copy-start | bytes 3145732
  85.2 110.9 %copy-start.2 = (bf16[256,512]{1,0:T(8,128)(2,1)S(1)}, bf16[256,512]{1,0:T(8,128)(2,1)}, u32[]{:S(2)}) copy-start(bf16[256,512]{1,0:T(8,128)(2,1)} %param.13) | copy-start | bytes 786436
  172.4 42.3 %all-gather.16.cloned.1.call-start = ((), (), s32[]{:S(2)}) async-start(), calls=%async_computation.7 | async-start | bytes 1310720 | tf_op jit(solution)/shard_map/all_gather | solution.py:108
  197.9 168.1 %all-gather.18.cloned.1.call-start = ((), (), s32[]{:S(2)}) async-start(), calls=%async_computation.8 | async-start | bytes 10485760 | tf_op jit(solution)/shard_map/all_gather | solution.py:113
  198.6 316.7 %copy-start.7 = (f32[2048]{0:T(1024)S(1)}, f32[2048]{0:T(1024)}, u32[]{:S(2)}) copy-start(f32[2048]{0:T(1024)} %param.15) | copy-start | bytes 24580
  198.6 316.7 %all-gather.20.cloned.1.call-start = ((), (), s32[]{:S(2)}) async-start(), calls=%async_computation.9 | async-start | bytes 10485760 | tf_op jit(solution)/shard_map/all_gather | solution.py:120
  199.4 350.7 %reduce-scatter.5.cloned.1.call-start = ((), (), s32[]{:S(2)}) async-start(), calls=%async_computation.10 | async-start | bytes 1310720 | tf_op jit(solution)/shard_map/reduce_scatter | solution.py:123
  216.3 333.8 %copy-start.1 = (bf16[256,512]{1,0:T(8,128)(2,1)S(1)}, bf16[256,512]{1,0:T(8,128)(2,1)}, u32[]{:S(2)}) copy-start(bf16[256,512]{1,0:T(8,128)(2,1)} %add_convert_fusion.1) | copy-start | bytes 786436
Sparse Core Ops, SparseCore 0:
  8.9 19.4 all-gather.7
  29.9 45.6 all-gather.9
  77.2 44.4 all-gather.11
  123.1 44.4 all-gather.13
  172.5 23.5 reduce-scatter.2
  198.0 16.6 all-gather.15
  216.3 149.6 all-gather.17
  367.5 147.7 all-gather.19
  527.1 22.9 reduce-scatter.4
where the time goes:
time: 559 us; the launch traced here: 558 us
  waiting for transfers between devices  511 us (91%)
  matrix products  19.7 us (4%)
  between operations  13.8 us (2%)
  other arithmetic  9.49 us (2%)
    all_gather x1, waiting for transfers between devices, per_device(): lax.all_gather(up_projection_weight, 'fs', axis=0, tiled=True)  150 us
    all_gather x1, waiting for transfers between devices, per_device(): lax.all_gather(down_projection_weight, 'fs', axis=1, tiled=True)  149 us
    all_gather x1, waiting for transfers between devices, per_device(): lax.all_gather(output_projection_weight, 'fs', axis=1, tiled=True)  45.9 us
    all_gather x1, waiting for transfers between devices, per_device(): lax.all_gather(recurrent_projection_weight, 'fs', axis=0, tiled=True)  45.7 us
    all_gather x1, waiting for transfers between devices, per_device(): lax.all_gather(gate_projection_weight, 'fs', axis=0, tiled=True)  36.4 us
    reduce_scatter x1, waiting for transfers between devices, per_device(): lax.psum_scatter(partials.astype(jnp.bfloat16), 'tp', scatter_dimension=1...  23.7 us
    reduce_scatter x1, waiting for transfers between devices, per_device(): lax.psum_scatter(down_terms.astype(jnp.bfloat16), 'tp', scatter_dimension...  23.1 us
    all_gather x1, waiting for transfers between devices, per_device(): whole_rows = lax.all_gather(tokens, 'tp', axis=1, tiled=True)  17.4 us
  transfers between devices with their start and end apart: 9, of which 9 were waited for; matrix products, arithmetic and copies ran while one was open for 2% of the time, Pallas kernels for 0%

commit v1 on v0

--- a/solution.py
+++ b/solution.py
@@ -2,6 +2,24 @@
 import jax.numpy as jnp
 from jax import lax
 from jax.sharding import PartitionSpec as P
+
+
+def ring_gather(shard, axis, dim):
+    ways, here, turn = (lax.axis_size(axis), lax.axis_index(axis), shard.shape[dim])
+    dims = [n * ways if d == dim else n for d, n in enumerate(shard.shape)]
+    full = lax.dynamic_update_slice_in_dim(
+        jnp.zeros(dims, shard.dtype), shard, here * turn, axis=dim
+    )
+    going_up = going_down = shard
+    for far in range(1, ways // 2 + 1):
+        going_up = lax.ppermute(going_up, axis, [(d, (d + 1) % ways) for d in range(ways)])
+        full = lax.dynamic_update_slice_in_dim(full, going_up, (here - far) % ways * turn, axis=dim)
+        if 2 * far < ways:
+            going_down = lax.ppermute(going_down, axis, [(d, (d - 1) % ways) for d in range(ways)])
+            full = lax.dynamic_update_slice_in_dim(
+                full, going_down, (here + far) % ways * turn, axis=dim
+            )
+    return full
 
 
 def rms_rows(values_in, norm_gain):
@@ -109,9 +127,7 @@
     channel_in = rms_rows(middle, feedforward_norm_gain)
     columns = channel_in
     upward = jnp.dot(
-        columns,
-        lax.all_gather(up_projection_weight, "fs", axis=0, tiled=True),
-        preferred_element_type=jnp.float32,
+        columns, ring_gather(up_projection_weight, "fs", 0), preferred_element_type=jnp.float32
     )
     positive = jnp.maximum(upward, 0.0)
     squared = (positive * positive).astype(jnp.bfloat16)

time: 559 us -> 518 us (0.927)
  waiting for transfers between devices: 511 us -> 407 us
  starting transfers between devices: 0.31 us -> 47.8 us
  local copies, waits for them, and re-layouts: 4.25 us -> 19.6 us
    ppermute x0 -> x3, waiting for transfers between devices: none -> 188 us  [the longest x2 101 us: ring_gather(): lax.ppermute(going_up, axis, [(d, (d + 1) % ways) for d in range(ways)])]
    all_gather x1 -> x0, waiting for transfers between devices: 150 us -> none  [per_device(): lax.all_gather(up_projection_weight, 'fs', axis=0, tiled=True)]
    all_gather x1, waiting for transfers between devices: 149 us -> 21.8 us  [per_device(): lax.all_gather(down_projection_weight, 'fs', axis=1, tiled=True)]
    ppermute x0 -> x3, starting transfers between devices: none -> 47.5 us  [the longest x2 45.1 us: ring_gather(): lax.ppermute(going_up, axis, [(d, (d + 1) % ways) for d in range(ways)])]
    all_gather x1, waiting for transfers between devices: 15.3 us -> 0.01 us  [per_device(): middle = lax.all_gather(residual, 'tp', axis=1, tiled=True)]
    dynamic_update_slice x0 -> x4, local copies, waits for them, and re-layouts: none -> 11 us  [the longest x2 6.33 us: ring_gather(): lax.dynamic_update_slice_in_dim(full, going_up, (here - far) % ways * tur...]
  transfers between devices with their start and end apart: 9 -> 11, of which waited for: 9 -> 10; matrix products, arithmetic and copies ran while one was open for 2% -> 6% of each run, Pallas kernels for 0% -> 0%
where the time goes in v1:
time: 518 us
  waiting for transfers between devices  407 us (79%)
  starting transfers between devices  47.8 us (9%)
  matrix products  19.8 us (4%)
  local copies, waits for them, and re-layouts  19.6 us (4%)
  between operations  14.1 us (3%)
  other arithmetic  9.49 us (2%)
    ppermute x2, waiting for transfers between devices, ring_gather(): lax.ppermute(going_up, axis, [(d, (d + 1) % ways) for d in range(ways)])  101 us
    ppermute x1, waiting for transfers between devices, ring_gather(): lax.ppermute(going_down, axis, [(d, (d - 1) % ways) for d in range(ways)])  87 us
    all_gather x1, waiting for transfers between devices, per_device(): lax.all_gather(output_projection_weight, 'fs', axis=1, tiled=True)  45.9 us
    all_gather x1, waiting for transfers between devices, per_device(): lax.all_gather(recurrent_projection_weight, 'fs', axis=0, tiled=True)  45.7 us
    ppermute x2, starting transfers between devices, ring_gather(): lax.ppermute(going_up, axis, [(d, (d + 1) % ways) for d in range(ways)])  45.1 us
    all_gather x1, waiting for transfers between devices, per_device(): lax.all_gather(gate_projection_weight, 'fs', axis=0, tiled=True)  36.4 us
    reduce_scatter x1, waiting for transfers between devices, per_device(): lax.psum_scatter(down_terms.astype(jnp.bfloat16), 'tp', scatter_dimension...  24.7 us
    reduce_scatter x1, waiting for transfers between devices, per_device(): lax.psum_scatter(partials.astype(jnp.bfloat16), 'tp', scatter_dimension=1...  23.7 us
  transfers between devices with their start and end apart: 11, of which 10 were waited for; matrix products, arithmetic and copies ran while one was open for 6% of the time, Pallas kernels for 0%

profile of v1, /device:TPU:0, one launch (start us, length us, event | category | flops | bytes accessed | tf_op | source)
XLA Modules:
  0.0 517.7 jit_solution(7174164210562795546)
XLA Ops:
  6.5 0.7 all-gather.7.cloned.1.call-update
  7.3 0.0 all-gather.9.cloned.1.call-start
  7.3 0.7 all-gather.9.cloned.1.call-update
  8.0 0.0 all-gather.11.cloned.1.call-start
  8.1 0.7 all-gather.11.cloned.1.call-update
  8.7 0.0 all-gather.13.cloned.1.call-start
  8.8 0.5 all-gather.13.cloned.1.call-update
  9.3 0.0 reduce-scatter.3.cloned.1.call-start
  9.4 0.8 slice_convert_fusion.3
  10.2 0.7 fusion.55
  10.9 17.4 %all-gather.7.cloned.1.call-done = bf16[256,2048]{1,0:T(8,128)(2,1)} async-done(((bf16[256,512]{1,0:T(8,128)(2,1)}), bf16[256,2048]{1,0:T(8,128)(2,1)}) %all-gather.7.cloned.1.call-update) | async-done | bytes 1048592 | tf_op jit(solution)/shard_map/all_gather | solution.py:91
  28.4 1.5 fusion.2
  29.9 45.7 %all-gather.9.cloned.1.call-done = bf16[2048,512]{1,0:T(8,128)(2,1)} async-done(((bf16[512,512]{1,0:T(8,128)(2,1)}), bf16[2048,512]{1,0:T(8,128)(2,1)}) %all-gather.9.cloned.1.call-update) | async-done | bytes 2097168 | tf_op jit(solution)/shard_map/all_gather | solution.py:101
  75.6 2.7 fusion.14
  78.3 0.2 fusion.77
  78.6 0.3 fusion.11
  78.9 0.2 copy.22
  79.1 0.1 copy-done.6
  79.2 0.3 fusion.13
  79.6 0.2 copy.23
  79.8 0.7 fusion.29
  80.4 0.3 slice.215
  80.8 0.3 slice.216
  81.1 0.3 slice.214
  81.4 0.3 slice.218
  81.8 0.1 fusion.62
  81.9 0.1 slice.221
  82.0 0.1 slice.222
  82.1 0.1 slice.220
  82.2 0.1 slice.224
  83.1 0.2 slice.219
  83.3 0.2 slice.268
  83.5 0.3 slice.270
  83.9 0.3 slice.213
  85.0 0.1 pad.69
  85.0 0.1 fusion.41
  85.2 0.1 pad.68
  85.2 36.4 %all-gather.11.cloned.1.call-done = bf16[2048,512]{1,0:T(8,128)(2,1)} async-done(((bf16[512,512]{1,0:T(8,128)(2,1)}), bf16[2048,512]{1,0:T(8,128)(2,1)}) %all-gather.11.cloned.1.call-update) | async-done | bytes 2097168 | tf_op jit(solution)/shard_map/all_gather | solution.py:96
  121.7 45.9 %all-gather.13.cloned.1.call-done = bf16[512,2048]{1,0:T(8,128)(2,1)} async-done(((bf16[512,512]{1,0:T(8,128)(2,1)}), bf16[512,2048]{1,0:T(8,128)(2,1)}) %all-gather.13.cloned.1.call-update) | async-done | bytes 2097168 | tf_op jit(solution)/shard_map/all_gather | solution.py:117
  167.6 4.8 convolution_convert_fusion
  172.4 0.0 reduce-scatter.3.cloned.1.call-update
  172.4 0.0 all-gather.15.cloned.1.call-start
  172.5 23.7 %reduce-scatter.3.cloned.1.call-done = bf16[256,512]{1,0:T(8,128)(2,1)} async-done(((bf16[256,2048]{1,0:T(8,128)(2,1)}), bf16[256,512]{1,0:T(8,128)(2,1)}) %reduce-scatter.3.cloned.1.call-update) | async-done | bytes 262160 | tf_op jit(solution)/shard_map/reduce_scatter | solution.py:122
  196.2 1.7 add_convert_fusion.1
  197.9 0.0 all-gather.15.cloned.1.call-update
  197.9 0.0 all-gather.17.cloned.1.call-start
  198.0 0.7 all-gather.17.cloned.1.call-update
  198.7 0.0 reduce-scatter.5.cloned.1.call-start
  198.7 1.5 collective-permute-start
  200.3 2.3 collective-permute-start.1
  202.6 65.4 %collective-permute-done = bf16[512,2048]{1,0:T(8,128)(2,1)} collective-permute-done((bf16[512,2048]{1,0:T(8,128)(2,1)S(1)}, bf16[512,2048]{1,0:T(8,128)(2,1)}, u32[]{:S(2)}, u32[]{:S(2)}) %collective-permute-start) | collective-permute-done | bytes 2097184 | tf_op jit(solution)/shard_map/ppermute | solution.py:15
  268.0 43.6 %collective-permute-start.2 = (bf16[512,2048]{1,0:T(8,128)(2,1)}, bf16[512,2048]{1,0:T(8,128)(2,1)}, u32[]{:S(2)}, u32[]{:S(2)}) collective-permute-start(bf16[512,2048]{1,0:T(8,128)(2,1)} %collective-permute-done), channel_id=1, source_target_pairs={{0,4},{4,8},{8,12},{12,0},{1,5},{5,9},{9,13},{13,1},{2,6},{6,10},{... | collective-permute-start | bytes 6291464 | tf_op jit(solution)/shard_map/ppermute | solution.py:15
  311.6 4.3 broadcast_in_dim.2
  315.9 1.5 constant_dynamic-update-slice_fusion.3
  317.4 3.2 constant_dynamic-update-slice_fusion.2
  320.6 87.0 %collective-permute-done.1 = bf16[512,2048]{1,0:T(8,128)(2,1)} collective-permute-done((bf16[512,2048]{1,0:T(8,128)(2,1)S(1)}, bf16[512,2048]{1,0:T(8,128)(2,1)}, u32[]{:S(2)}, u32[]{:S(2)}) %collective-permute-start.1) | collective-permute-done | bytes 2097184 | tf_op jit(solution)/shard_map/ppermute | solution.py:18
  407.6 3.2 constant_dynamic-update-slice_fusion.1
  410.8 35.7 %collective-permute-done.2 = bf16[512,2048]{1,0:T(8,128)(2,1)} collective-permute-done((bf16[512,2048]{1,0:T(8,128)(2,1)}, bf16[512,2048]{1,0:T(8,128)(2,1)}, u32[]{:S(2)}, u32[]{:S(2)}) %collective-permute-start.2) | collective-permute-done | bytes 2097184 | tf_op jit(solution)/shard_map/ppermute | solution.py:15
  446.4 3.1 constant_dynamic-update-slice_fusion
  449.6 1.5 fusion.5
  451.1 21.8 %all-gather.17.cloned.1.call-done = bf16[2048,2048]{1,0:T(8,128)(2,1)} async-done(((bf16[2048,512]{1,0:T(8,128)(2,1)}), bf16[2048,2048]{1,0:T(8,128)(2,1)}) %all-gather.17.cloned.1.call-update) | async-done | bytes 8388624 | tf_op jit(solution)/shard_map/all_gather | solution.py:136
  472.9 11.6 %convolution_convert_fusion.1 = bf16[256,2048]{1,0:T(8,128)(2,1)} fusion(bf16[2048,2048]{1,0:T(8,128)(2,1)} %all-gather.17.cloned.1.call-done, bf16[2048,2048]{1,0:T(8,128)(2,1)} %constant_dynamic-update-slice_fusion, bf16[256,2048]{1,0:T(8,128)(2,1)} %all-gather.15.cloned.1.call-done, f32[2048]{0:T(1024)S(1)} %copy-done.8, f32[256]{0:T(256)S(1)} %add_rsqrt_fusion), kind=kOutput, calls=%fused_computation.8 | convolution fusion | flops 4299161600 | bytes 18883584 | tf_op jit(solution)/shard_map/dot_general | solution.py:134
  484.5 24.7 %reduce-scatter.5.cloned.1.call-done = bf16[256,512]{1,0:T(8,128)(2,1)} async-done(((bf16[256,2048]{1,0:T(8,128)(2,1)}), bf16[256,512]{1,0:T(8,128)(2,1)}) %reduce-scatter.5.cloned.1.call-update) | async-done | bytes 262160 | tf_op jit(solution)/shard_map/reduce_scatter | solution.py:139
  509.2 1.7 add_convert_fusion
  (95 shorter events, 1.3 us)
Async XLA Ops:
  6.5 72.0 %copy-start = (bf16[4,128,128]{2,1,0:T(8,128)(2,1)S(1)}, bf16[4,128,128]{2,1,0:T(8,128)(2,1)}, u32[]{:S(2)}) copy-start(bf16[4,128,128]{2,1,0:T(8,128)(2,1)} %param.19) | copy-start | bytes 393220
  6.5 69.1 %copy-start.7 = (f32[2048]{0:T(1024)S(1)}, f32[2048]{0:T(1024)}, u32[]{:S(2)}) copy-start(f32[2048]{0:T(1024)} %param.14) | copy-start | bytes 24580
  6.5 21.8 %all-gather.7.cloned.1.call-start = ((), (), s32[]{:S(2)}) async-start(), calls=%async_computation.2 | async-start | bytes 1310720 | tf_op jit(solution)/shard_map/all_gather | solution.py:91
  7.3 68.3 %all-gather.9.cloned.1.call-start = ((), (), s32[]{:S(2)}) async-start(), calls=%async_computation.3 | async-start | bytes 2621440 | tf_op jit(solution)/shard_map/all_gather | solution.py:101
  8.0 113.7 %all-gather.11.cloned.1.call-start = ((), (), s32[]{:S(2)}) async-start(), calls=%async_computation.4 | async-start | bytes 2621440 | tf_op jit(solution)/shard_map/all_gather | solution.py:96
  8.7 158.9 %all-gather.13.cloned.1.call-start = ((), (), s32[]{:S(2)}) async-start(), calls=%async_computation.5 | async-start | bytes 2621440 | tf_op jit(solution)/shard_map/all_gather | solution.py:117
  9.3 186.9 %reduce-scatter.3.cloned.1.call-start = ((), (), s32[]{:S(2)}) async-start(), calls=%async_computation.6 | async-start | bytes 1310720 | tf_op jit(solution)/shard_map/reduce_scatter | solution.py:122
  78.3 0.9 copy-start.6
  78.9 0.8 copy-start.5
  84.9 82.7 %copy-start.4 = (bf16[256,2048]{1,0:T(8,128)(2,1)S(1)}, bf16[256,2048]{1,0:T(8,128)(2,1)}, u32[]{:S(2)}) copy-start(bf16[256,2048]{1,0:T(8,128)(2,1)} %all-gather.7.cloned.1.call-done) | copy-start | bytes 3145732
  85.2 111.0 %copy-start.3 = (bf16[256,512]{1,0:T(8,128)(2,1)S(1)}, bf16[256,512]{1,0:T(8,128)(2,1)}, u32[]{:S(2)}) copy-start(bf16[256,512]{1,0:T(8,128)(2,1)} %param.13) | copy-start | bytes 786436
  172.4 26.3 %copy-start.2 = (bf16[512,2048]{1,0:T(8,128)(2,1)S(1)}, bf16[512,2048]{1,0:T(8,128)(2,1)}, u32[]{:S(2)}) copy-start(bf16[512,2048]{1,0:T(8,128)(2,1)} %param.24) | copy-start | bytes 6291460
  172.4 277.2 %all-gather.15.cloned.1.call-start = ((), (), s32[]{:S(2)}) async-start(), calls=%async_computation.7 | async-start | bytes 1310720 | tf_op jit(solution)/shard_map/all_gather | solution.py:126
  197.9 275.0 %all-gather.17.cloned.1.call-start = ((), (), s32[]{:S(2)}) async-start(), calls=%async_computation.8 | async-start | bytes 10485760 | tf_op jit(solution)/shard_map/all_gather | solution.py:136
  198.7 310.5 %reduce-scatter.5.cloned.1.call-start = ((), (), s32[]{:S(2)}) async-start(), calls=%async_computation.9 | async-start | bytes 1310720 | tf_op jit(solution)/shard_map/reduce_scatter | solution.py:139
  198.7 69.2 %collective-permute-start = (bf16[512,2048]{1,0:T(8,128)(2,1)S(1)}, bf16[512,2048]{1,0:T(8,128)(2,1)}, u32[]{:S(2)}, u32[]{:S(2)}) collective-permute-start(bf16[512,2048]{1,0:T(8,128)(2,1)S(1)} %copy-done.2), channel_id=1, source_target_pairs={{0,4},{4,8},{8,12},{12,0},{1,5},{5,9},{9,13},{13,1},{2,6},{6,10},{... | collective-permute-start | bytes 6291464 | tf_op jit(solution)/shard_map/ppermute | solution.py:15
  200.3 207.3 %collective-permute-start.1 = (bf16[512,2048]{1,0:T(8,128)(2,1)S(1)}, bf16[512,2048]{1,0:T(8,128)(2,1)}, u32[]{:S(2)}, u32[]{:S(2)}) collective-permute-start(bf16[512,2048]{1,0:T(8,128)(2,1)S(1)} %copy-done.2), channel_id=1, source_target_pairs={{0,12},{4,0},{8,4},{12,8},{1,13},{5,1},{9,5},{13,9},{2,14},{6,2},{... | collective-permute-start | bytes 6291464 | tf_op jit(solution)/shard_map/ppermute | solution.py:18
  268.0 178.5 %collective-permute-start.2 = (bf16[512,2048]{1,0:T(8,128)(2,1)}, bf16[512,2048]{1,0:T(8,128)(2,1)}, u32[]{:S(2)}, u32[]{:S(2)}) collective-permute-start(bf16[512,2048]{1,0:T(8,128)(2,1)} %collective-permute-done), channel_id=1, source_target_pairs={{0,4},{4,8},{8,12},{12,0},{1,5},{5,9},{9,13},{13,1},{2,6},{6,10},{... | collective-permute-start | bytes 6291464 | tf_op jit(solution)/shard_map/ppermute | solution.py:15
  410.8 62.1 %copy-start.8 = (f32[2048]{0:T(1024)S(1)}, f32[2048]{0:T(1024)}, u32[]{:S(2)}) copy-start(f32[2048]{0:T(1024)} %param.15) | copy-start | bytes 24580
  451.1 58.1 %copy-start.1 = (bf16[256,512]{1,0:T(8,128)(2,1)S(1)}, bf16[256,512]{1,0:T(8,128)(2,1)}, u32[]{:S(2)}) copy-start(bf16[256,512]{1,0:T(8,128)(2,1)} %add_convert_fusion.1) | copy-start | bytes 786436
Sparse Core Ops, SparseCore 0:
  8.9 19.4 all-gather.6
  29.9 45.6 all-gather.8
  77.2 44.4 all-gather.10
  123.1 44.4 all-gather.12
  172.5 23.6 reduce-scatter.2
  198.0 16.6 all-gather.14
  216.4 256.4 all-gather.16
  484.6 24.4 reduce-scatter.4
